TPU v7x, 32 devices: a whole 2x2x4 slice. The times are simulated.
32 devices in a mesh: grp: 2 (over x), fs: 4 (over z), tp: 4 (over y, core).
Axes of the slice: x: 2, y: 2, z: 4, core: 2. Of those that a mesh axis runs over, the one named last changes fastest.
Arguments:
- stream: bfloat16 [2048, 2048], P(('grp', 'fs'), 'tp'), parts along dimension 0, may hold values from -80 to 80
- mixed: bfloat16 [2048, 2048], P(('grp', 'fs'), 'tp'), parts along dimension 0, may hold values from -6 to 6
- out_weight: bfloat16 [2048, 2048], P('fs', 'tp'), may hold values from -0.125 to 0.125
- norm_gain: bfloat16 [2048], P('tp'), may hold values from 0.099609375 to 1.8984375
- up_weight: bfloat16 [2048, 8192], P('fs', 'tp'), may hold values from -0.125 to 0.125
- down_weight: bfloat16 [8192, 2048], P('tp', 'fs'), may hold values from -0.09375 to 0.09375
Outputs:
- result: bfloat16 [2048, 2048], P(('grp', 'fs'), 'tp'), parts along dimension 0
There are 2 independent parts, one for each index of `grp`. A program takes and returns all parts, laid end to end along the dimension named above; an argument that names none is the same for every part. Nothing has to cross between parts.
All inputs are finite; a program needn't handle non-finite values.
Results may differ from a plain program's by a relative error of at most 0.01.
Values may be sent and summed in bfloat16 or wider, within the bound.
A program may use at most 64 MiB of HBM per device.

v0:
```python
import jax
import jax.numpy as jnp
from jax import lax
from jax.sharding import PartitionSpec as P

epsilon = 1e-06


def fold_product(left, portion):
    return jnp.dot(left, portion, preferred_element_type=jnp.float32)


def body(stream, mixed, out_weight, norm_gain, up_weight, down_weight):
    mixed_whole = lax.all_gather(mixed, "tp", axis=1, tiled=True)
    projected = fold_product(mixed_whole, lax.all_gather(out_weight, "fs", axis=0, tiled=True))
    resid = (stream.astype(jnp.float32) + projected).astype(jnp.bfloat16)
    widened = resid.astype(jnp.float32)
    resid_whole, gain_whole = (
        lax.all_gather(resid, "tp", axis=1, tiled=True),
        lax.all_gather(norm_gain, "tp", axis=0, tiled=True),
    )
    stream_wide = resid_whole.astype(jnp.float32)
    energy = jnp.mean(stream_wide * stream_wide, axis=1, keepdims=True)
    normed_whole = (
        stream_wide * lax.rsqrt(energy + epsilon) * gain_whole.astype(jnp.float32)
    ).astype(jnp.bfloat16)
    up_full = lax.all_gather(up_weight, "fs", axis=0, tiled=True)
    up_values = jnp.dot(normed_whole, up_full, preferred_element_type=jnp.float32)
    activated = jnp.square(jax.nn.relu(up_values)).astype(jnp.bfloat16)
    partials = jnp.dot(
        activated,
        lax.all_gather(down_weight, "fs", axis=1, tiled=True),
        preferred_element_type=jnp.float32,
    )
    branch = lax.psum_scatter(partials, "tp", scatter_dimension=1, tiled=True)
    return (widened + branch).astype(jnp.bfloat16)


def solution(mesh):
    placed = (
        P(("grp", "fs"), "tp"),
        P(("grp", "fs"), "tp"),
        P("fs", "tp"),
        P("tp"),
        P("fs", "tp"),
        P("tp", "fs"),
    )
    return jax.shard_map(
        body, mesh=mesh, in_specs=placed, out_specs=P(("grp", "fs"), "tp"), check_vma=False
    )
```

profile of v0, /device:TPU:0, one launch (start us, length us, event | category | flops | bytes accessed | tf_op | source)
XLA Modules:
  0.0 445.1 jit_solution(17761984811447888567)
XLA Ops:
  6.5 0.0 all-gather.7.cloned.1.call-start
  6.5 0.7 all-gather.7.cloned.1.call-update
  7.3 0.0 all-gather.9.cloned.1.call-start
  7.3 0.7 all-gather.9.cloned.1.call-update
  8.0 0.0 all-gather.11.cloned.1.call-start
  8.1 20.3 %all-gather.7.cloned.1.call-done = bf16[256,2048]{1,0:T(8,128)(2,1)} async-done(((bf16[256,512]{1,0:T(8,128)(2,1)}), bf16[256,2048]{1,0:T(8,128)(2,1)}) %all-gather.7.cloned.1.call-update) | async-done | bytes 1048592 | tf_op jit(solution)/shard_map/all_gather | solution.py:14
  28.4 47.3 %all-gather.9.cloned.1.call-done = bf16[2048,512]{1,0:T(8,128)(2,1)} async-done(((bf16[512,512]{1,0:T(8,128)(2,1)}), bf16[2048,512]{1,0:T(8,128)(2,1)}) %all-gather.9.cloned.1.call-update) | async-done | bytes 2097168 | tf_op jit(solution)/shard_map/all_gather | solution.py:15
  75.6 3.3 fusion.5
  78.9 0.0 all-gather.11.cloned.1.call-update
  78.9 0.0 copy-start.1
  78.9 0.0 all-gather.13.cloned.1.call-start
  79.0 0.5 all-gather.13.cloned.1.call-update
  79.5 0.0 all-gather.15.cloned.1.call-start
  79.6 0.5 all-gather.15.cloned.1.call-update
  80.1 0.0 reduce-scatter.2.cloned.1.call-start
  80.2 0.0 copy-done.1
  80.2 5.2 %all-gather = bf16[4,1,512]{2,1,0:T(2,128)(2,1)S(1)} all-gather(bf16[1,1,512]{2,1,0:T(2,128)(2,1)S(1)} %reshape.9), channel_id=1, replica_groups=mesh['grp'=2,'fs'=4,'tp'=4] {'tp'}, dimensions={0}, use_global_device_ids=true | all-gather | bytes 5120 | tf_op jit(solution)/shard_map/all_gather | solution.py:20
  85.4 9.2 %all-gather.11.cloned.1.call-done = bf16[256,2048]{1,0:T(8,128)(2,1)} async-done(((bf16[256,512]{1,0:T(8,128)(2,1)}), bf16[256,2048]{1,0:T(8,128)(2,1)}) %all-gather.11.cloned.1.call-update) | async-done | bytes 1048592 | tf_op jit(solution)/shard_map/all_gather | solution.py:19
  94.6 1.5 fusion.2
  96.1 149.5 %all-gather.13.cloned.1.call-done = bf16[2048,2048]{1,0:T(8,128)(2,1)} async-done(((bf16[512,2048]{1,0:T(8,128)(2,1)}), bf16[2048,2048]{1,0:T(8,128)(2,1)}) %all-gather.13.cloned.1.call-update) | async-done | bytes 8388624 | tf_op jit(solution)/shard_map/all_gather | solution.py:27
  245.7 149.2 %all-gather.15.cloned.1.call-done = bf16[2048,2048]{1,0:T(8,128)(2,1)} async-done(((bf16[2048,512]{1,0:T(8,128)(2,1)}), bf16[2048,2048]{1,0:T(8,128)(2,1)}) %all-gather.15.cloned.1.call-update) | async-done | bytes 8388624 | tf_op jit(solution)/shard_map/all_gather | solution.py:32
  394.9 11.9 %fusion.10 = f32[256,2048]{1,0:T(8,128)} fusion(bf16[2048,2048]{1,0:T(8,128)(2,1)} %all-gather.15.cloned.1.call-done, bf16[2048,2048]{1,0:T(8,128)(2,1)} %all-gather.13.cloned.1.call-done, bf16[256,2048]{1,0:T(8,128)(2,1)} %all-gather.11.cloned.1.call-done, f32[2048]{0:T(1024)S(1)} %bitcast.5, f32[256]{0:T(256)S(1)} %add_rsqrt_fusion), kind=kOutput, calls=%fused_computation.12 | convolution fusion | flops 4298637312 | bytes 19932160 | tf_op jit(solution)/shard_map/dot_general | solution.py:30
  406.9 0.0 copy-start
  406.9 0.0 reduce-scatter.2.cloned.1.call-update
  406.9 29.5 %reduce-scatter.2.cloned.1.call-done = f32[256,512]{1,0:T(8,128)} async-done(((f32[256,2048]{1,0:T(8,128)}), f32[256,512]{1,0:T(8,128)}) %reduce-scatter.2.cloned.1.call-update) | async-done | bytes 524304 | tf_op jit(solution)/shard_map/reduce_scatter | solution.py:35
  436.4 0.0 copy-done
  436.4 1.8 add_convert_fusion
  (3 shorter events, 0.0 us)
Async XLA Ops:
  6.5 21.8 %all-gather.7.cloned.1.call-start = ((), (), s32[]{:S(2)}) async-start(), calls=%async_computation.1 | async-start | bytes 1310720 | tf_op jit(solution)/shard_map/all_gather | solution.py:14
  7.3 68.3 %all-gather.9.cloned.1.call-start = ((), (), s32[]{:S(2)}) async-start(), calls=%async_computation.2 | async-start | bytes 2621440 | tf_op jit(solution)/shard_map/all_gather | solution.py:15
  8.0 86.6 %all-gather.11.cloned.1.call-start = ((), (), s32[]{:S(2)}) async-start(), calls=%async_computation.3 | async-start | bytes 1310720 | tf_op jit(solution)/shard_map/all_gather | solution.py:19
  78.9 1.2 copy-start.1
  78.9 166.7 %all-gather.13.cloned.1.call-start = ((), (), s32[]{:S(2)}) async-start(), calls=%async_computation.4 | async-start | bytes 10485760 | tf_op jit(solution)/shard_map/all_gather | solution.py:27
  79.5 315.4 %all-gather.15.cloned.1.call-start = ((), (), s32[]{:S(2)}) async-start(), calls=%async_computation.5 | async-start | bytes 10485760 | tf_op jit(solution)/shard_map/all_gather | solution.py:32
  80.1 356.3 %reduce-scatter.2.cloned.1.call-start = ((), (), s32[]{:S(2)}) async-start(), calls=%async_computation.6 | async-start | bytes 2621440 | tf_op jit(solution)/shard_map/reduce_scatter | solution.py:35
  406.9 29.6 %copy-start = (bf16[256,512]{1,0:T(8,128)(2,1)S(1)}, bf16[256,512]{1,0:T(8,128)(2,1)}, u32[]{:S(2)}) copy-start(bf16[256,512]{1,0:T(8,128)(2,1)} %fusion.5) | copy-start | bytes 786436
Sparse Core Ops, SparseCore 0:
  8.9 19.4 all-gather.6
  29.9 45.6 all-gather.8
  79.1 15.4 all-gather.10
  96.0 149.5 all-gather.12
  247.1 147.7 all-gather.14
  407.0 29.3 reduce-scatter.1
where the time goes:
time: 445 us
  waiting for transfers between devices  408 us (92%)
  matrix products  15.3 us (3%)
  between operations  13.5 us (3%)
  blocking collectives  5.19 us (1%)
    all_gather x1, waiting for transfers between devices, body(): up_full = lax.all_gather(up_weight, 'fs', axis=0, tiled=True)  150 us
    all_gather x1, waiting for transfers between devices, body(): lax.all_gather(down_weight, 'fs', axis=1, tiled=True)  149 us
    all_gather x1, waiting for transfers between devices, body(): lax.all_gather(out_weight, 'fs', axis=0, tiled=True)  47.3 us
    reduce_scatter x1, waiting for transfers between devices, body(): branch = lax.psum_scatter(partials, 'tp', scatter_dimension=1, tiled=True)  29.5 us
    all_gather x1, waiting for transfers between devices, body(): mixed_whole = lax.all_gather(mixed, 'tp', axis=1, tiled=True)  20.3 us
    dot_general x1, matrix products, body(): jnp.dot(activated, lax.all_gather(down_weight, 'fs', axis=1, tiled=True),...  11.9 us
    all_gather x1, waiting for transfers between devices, body(): lax.all_gather(resid, 'tp', axis=1, tiled=True)  9.21 us
  transfers between devices with their start and end apart: 6, of which 6 were waited for; matrix products, arithmetic and copies ran while one was open for 0% of the time, Pallas kernels for 0%

commit v1 on v0

--- a/solution.py
+++ b/solution.py
@@ -4,6 +4,17 @@
 from jax.sharding import PartitionSpec as P
 
 epsilon = 1e-06
+
+
+def gather_by_hops(x, axis, dim):
+    size = lax.axis_size(axis)
+    right = [(i, (i + 1) % size) for i in range(size)]
+    parts = [x]
+    for stride in range(1, size):
+        parts = [lax.ppermute(parts[0], axis, right), *parts]
+    whole = jnp.concatenate(parts, axis=dim)
+    shift = (lax.axis_index(axis) + 1) * parts[-1].shape[dim]
+    return jnp.roll(whole, shift, axis=dim)
 
 
 def fold_product(left, portion):
@@ -24,7 +35,7 @@
     normed_whole = (
         stream_wide * lax.rsqrt(energy + epsilon) * gain_whole.astype(jnp.float32)
     ).astype(jnp.bfloat16)
-    up_full = lax.all_gather(up_weight, "fs", axis=0, tiled=True)
+    up_full = gather_by_hops(up_weight, "fs", 0)
     up_values = jnp.dot(normed_whole, up_full, preferred_element_type=jnp.float32)
     activated = jnp.square(jax.nn.relu(up_values)).astype(jnp.bfloat16)
     partials = jnp.dot(

time: 445 us -> 423 us (0.951)
  waiting for transfers between devices: 408 us -> 294 us
  starting transfers between devices: 0.2 us -> 70.3 us
  local copies, waits for them, and re-layouts: 0.01 us -> 21 us
    ppermute x0 -> x3, waiting for transfers between devices: none -> 195 us  [gather_by_hops(): parts = [lax.ppermute(parts[0], axis, right), *parts]]
    all_gather x1 -> x0, waiting for transfers between devices: 150 us -> none  [body(): up_full = lax.all_gather(up_weight, 'fs', axis=0, tiled=True)]
    all_gather x1, waiting for transfers between devices: 149 us -> 0.01 us  [body(): lax.all_gather(down_weight, 'fs', axis=1, tiled=True)]
    ppermute x0 -> x3, starting transfers between devices: none -> 70.1 us  [gather_by_hops(): parts = [lax.ppermute(parts[0], axis, right), *parts]]
    unnamed x5 -> x18, local copies, waits for them, and re-layouts: 0.01 us -> 19.4 us
    all_gather x1, waiting for transfers between devices: 9.21 us -> 0.02 us  [body(): lax.all_gather(resid, 'tp', axis=1, tiled=True)]
  transfers between devices with their start and end apart: 6 -> 8, of which waited for: 6 -> 6; matrix products, arithmetic and copies ran while one was open for 0% -> 5% of each run, Pallas kernels for 0% -> 0%
where the time goes in v1:
time: 423 us
  waiting for transfers between devices  294 us (70%)
  starting transfers between devices  70.3 us (17%)
  local copies, waits for them, and re-layouts  21 us (5%)
  matrix products  15.1 us (4%)
  between operations  13.2 us (3%)
  blocking collectives  5.18 us (1%)
    ppermute x3, waiting for transfers between devices, gather_by_hops(): parts = [lax.ppermute(parts[0], axis, right), *parts]  195 us
    ppermute x3, starting transfers between devices, gather_by_hops(): parts = [lax.ppermute(parts[0], axis, right), *parts]  70.1 us
    all_gather x1, waiting for transfers between devices, body(): lax.all_gather(out_weight, 'fs', axis=0, tiled=True)  47.3 us
    reduce_scatter x1, waiting for transfers between devices, body(): branch = lax.psum_scatter(partials, 'tp', scatter_dimension=1, tiled=True)  29.5 us
    all_gather x1, waiting for transfers between devices, body(): mixed_whole = lax.all_gather(mixed, 'tp', axis=1, tiled=True)  20.3 us
    unnamed x18, local copies, waits for them, and re-layouts  19.4 us
    dot_general x1, matrix products, body(): jnp.dot(activated, lax.all_gather(down_weight, 'fs', axis=1, tiled=True),...  11.8 us
  transfers between devices with their start and end apart: 8, of which 6 were waited for; matrix products, arithmetic and copies ran while one was open for 5% of the time, Pallas kernels for 0%

profile of v1, /device:TPU:0, one launch (start us, length us, event | category | flops | bytes accessed | tf_op | source)
XLA Modules:
  0.0 422.6 jit_solution(14289356904373567895)
XLA Ops:
  6.5 0.0 all-gather.6.cloned.1.call-start
  6.5 0.7 all-gather.6.cloned.1.call-update
  7.3 0.0 all-gather.8.cloned.1.call-start
  7.3 0.7 all-gather.8.cloned.1.call-update
  8.0 0.0 all-gather.10.cloned.1.call-start
  8.1 20.3 %all-gather.6.cloned.1.call-done = bf16[256,2048]{1,0:T(8,128)(2,1)} async-done(((bf16[256,512]{1,0:T(8,128)(2,1)}), bf16[256,2048]{1,0:T(8,128)(2,1)}) %all-gather.6.cloned.1.call-update) | async-done | bytes 1048592 | tf_op jit(solution)/shard_map/all_gather | solution.py:25
  28.4 47.3 %all-gather.8.cloned.1.call-done = bf16[2048,512]{1,0:T(8,128)(2,1)} async-done(((bf16[512,512]{1,0:T(8,128)(2,1)}), bf16[2048,512]{1,0:T(8,128)(2,1)}) %all-gather.8.cloned.1.call-update) | async-done | bytes 2097168 | tf_op jit(solution)/shard_map/all_gather | solution.py:26
  75.6 3.3 fusion.14
  78.9 0.0 copy-start
  78.9 0.0 all-gather.10.cloned.1.call-update
  78.9 0.0 all-gather.12.cloned.1.call-start
  79.0 0.5 all-gather.12.cloned.1.call-update
  79.5 0.0 reduce-scatter.2.cloned.1.call-start
  79.6 0.2 collective-permute-start
  79.8 69.2 %collective-permute-done = bf16[512,2048]{1,0:T(8,128)(2,1)S(1)} collective-permute-done((bf16[512,2048]{1,0:T(8,128)(2,1)}, bf16[512,2048]{1,0:T(8,128)(2,1)S(1)}, u32[]{:S(2)}, u32[]{:S(2)}) %collective-permute-start) | collective-permute-done | bytes 2097184 | tf_op jit(solution)/shard_map/ppermute | solution.py:14
  149.0 0.0 copy-start.1
  149.0 1.4 copy-done.1
  150.3 20.1 %collective-permute-start.1 = (bf16[512,2048]{1,0:T(8,128)(2,1)S(1)}, bf16[512,2048]{1,0:T(8,128)(2,1)}, u32[]{:S(2)}, u32[]{:S(2)}) collective-permute-start(bf16[512,2048]{1,0:T(8,128)(2,1)S(1)} %collective-permute-done), channel_id=1, source_target_pairs={{0,4},{4,8},{8,12},{12,0},{1,5},{5,9},{9,13},{13,1},{2,6},{6,10},{... | collective-permute-start | bytes 6291464 | tf_op jit(solution)/shard_map/ppermute | solution.py:14
  170.4 87.3 %collective-permute-done.1 = bf16[512,2048]{1,0:T(8,128)(2,1)} collective-permute-done((bf16[512,2048]{1,0:T(8,128)(2,1)S(1)}, bf16[512,2048]{1,0:T(8,128)(2,1)}, u32[]{:S(2)}, u32[]{:S(2)}) %collective-permute-start.1) | collective-permute-done | bytes 2097184 | tf_op jit(solution)/shard_map/ppermute | solution.py:14
  257.7 49.8 %collective-permute-start.2 = (bf16[512,2048]{1,0:T(8,128)(2,1)}, bf16[512,2048]{1,0:T(8,128)(2,1)}, u32[]{:S(2)}, u32[]{:S(2)}) collective-permute-start(bf16[512,2048]{1,0:T(8,128)(2,1)} %collective-permute-done.1), channel_id=1, source_target_pairs={{0,4},{4,8},{8,12},{12,0},{1,5},{5,9},{9,13},{13,1},{2,6},{6,10},{... | collective-permute-start | bytes 6291464 | tf_op jit(solution)/shard_map/ppermute | solution.py:14
  307.5 0.7 reshape.9
  308.2 5.2 %all-gather = bf16[4,1,512]{2,1,0:T(2,128)(2,1)S(1)} all-gather(bf16[1,1,512]{2,1,0:T(2,128)(2,1)S(1)} %reshape.9), channel_id=1, replica_groups=mesh['grp'=2,'fs'=4,'tp'=4] {'tp'}, dimensions={0}, use_global_device_ids=true | all-gather | bytes 5120 | tf_op jit(solution)/shard_map/all_gather | solution.py:31
  313.4 0.0 all-gather.10.cloned.1.call-done
  313.4 0.0 copy-start.2
  313.5 1.7 fusion.11
  315.1 38.9 %collective-permute-done.2 = bf16[512,2048]{1,0:T(8,128)(2,1)} collective-permute-done((bf16[512,2048]{1,0:T(8,128)(2,1)}, bf16[512,2048]{1,0:T(8,128)(2,1)}, u32[]{:S(2)}, u32[]{:S(2)}) %collective-permute-start.2) | collective-permute-done | bytes 2097184 | tf_op jit(solution)/shard_map/ppermute | solution.py:14
  354.0 3.2 constant_dynamic-update-slice_fusion.7
  357.2 3.2 constant_dynamic-update-slice_fusion.6
  360.3 0.0 copy-done.2
  360.3 1.5 constant_dynamic-update-slice_fusion.5
  361.8 0.0 copy-done
  361.8 1.6 constant_dynamic-update-slice_fusion.4
  363.4 0.0 copy-start.3
  363.4 3.3 constant_dynamic-update-slice_fusion.3
  366.7 3.2 constant_dynamic-update-slice_fusion.2
  369.9 1.5 constant_dynamic-update-slice_fusion.1
  371.4 1.6 constant_dynamic-update-slice_fusion
  372.9 0.0 all-gather.12.cloned.1.call-done
  372.9 0.0 copy-done.3
  373.0 0.0 copy-start.4
  373.0 11.8 %fusion.20 = f32[256,2048]{1,0:T(8,128)} fusion(bf16[2048,2048]{1,0:T(8,128)(2,1)} %all-gather.12.cloned.1.call-done, bf16[4096,2048]{1,0:T(8,128)(2,1)} %constant_dynamic-update-slice_fusion, s32[]{:T(128)S(6)} %select_n.14, bf16[256,2048]{1,0:T(8,128)(2,1)S(1)} %copy-done.3, f32[2048]{0:T(1024)S(1)} %bitcast.4, f32[256]{0:T(256)S(1)} %add_rsqrt_fusion), kind=kOutput, calls=%fused_computation.14 | convolution fusion | flops 4298637312 | bytes 19932164 | tf_op jit(solution)/shard_map/dot_general | solution.py:41
  384.7 0.0 reduce-scatter.2.cloned.1.call-update
  384.7 29.5 %reduce-scatter.2.cloned.1.call-done = f32[256,512]{1,0:T(8,128)} async-done(((f32[256,2048]{1,0:T(8,128)}), f32[256,512]{1,0:T(8,128)}) %reduce-scatter.2.cloned.1.call-update) | async-done | bytes 524304 | tf_op jit(solution)/shard_map/reduce_scatter | solution.py:46
  414.2 0.0 copy-done.4
  414.2 1.8 add_convert_fusion
  (2 shorter events, 0.0 us)
Async XLA Ops:
  6.5 21.8 %all-gather.6.cloned.1.call-start = ((), (), s32[]{:S(2)}) async-start(), calls=%async_computation.1 | async-start | bytes 1310720 | tf_op jit(solution)/shard_map/all_gather | solution.py:25
  7.3 68.3 %all-gather.8.cloned.1.call-start = ((), (), s32[]{:S(2)}) async-start(), calls=%async_computation.2 | async-start | bytes 2621440 | tf_op jit(solution)/shard_map/all_gather | solution.py:26
  8.0 305.4 %all-gather.10.cloned.1.call-start = ((), (), s32[]{:S(2)}) async-start(), calls=%async_computation.3 | async-start | bytes 1310720 | tf_op jit(solution)/shard_map/all_gather | solution.py:30
  78.9 282.9 %copy-start = (bf16[512,2048]{1,0:T(8,128)(2,1)S(1)}, bf16[512,2048]{1,0:T(8,128)(2,1)}, u32[]{:S(2)}) copy-start(bf16[512,2048]{1,0:T(8,128)(2,1)} %param.10) | copy-start | bytes 6291460
  78.9 294.0 %all-gather.12.cloned.1.call-start = ((), (), s32[]{:S(2)}) async-start(), calls=%async_computation.4 | async-start | bytes 10485760 | tf_op jit(solution)/shard_map/all_gather | solution.py:43
  79.5 334.7 %reduce-scatter.2.cloned.1.call-start = ((), (), s32[]{:S(2)}) async-start(), calls=%async_computation.5 | async-start | bytes 2621440 | tf_op jit(solution)/shard_map/reduce_scatter | solution.py:46
  79.6 69.4 %collective-permute-start = (bf16[512,2048]{1,0:T(8,128)(2,1)}, bf16[512,2048]{1,0:T(8,128)(2,1)S(1)}, u32[]{:S(2)}, u32[]{:S(2)}) collective-permute-start(bf16[512,2048]{1,0:T(8,128)(2,1)} %param.10), channel_id=1, source_target_pairs={{0,4},{4,8},{8,12},{12,0},{1,5},{5,9},{9,13},{13,1},{2,6},{6,10},{... | collective-permute-start | bytes 6291464 | tf_op jit(solution)/shard_map/ppermute | solution.py:14
  149.0 1.4 copy-start.1
  150.3 107.4 %collective-permute-start.1 = (bf16[512,2048]{1,0:T(8,128)(2,1)S(1)}, bf16[512,2048]{1,0:T(8,128)(2,1)}, u32[]{:S(2)}, u32[]{:S(2)}) collective-permute-start(bf16[512,2048]{1,0:T(8,128)(2,1)S(1)} %collective-permute-done), channel_id=1, source_target_pairs={{0,4},{4,8},{8,12},{12,0},{1,5},{5,9},{9,13},{13,1},{2,6},{6,10},{... | collective-permute-start | bytes 6291464 | tf_op jit(solution)/shard_map/ppermute | solution.py:14
  257.7 96.3 %collective-permute-start.2 = (bf16[512,2048]{1,0:T(8,128)(2,1)}, bf16[512,2048]{1,0:T(8,128)(2,1)}, u32[]{:S(2)}, u32[]{:S(2)}) collective-permute-start(bf16[512,2048]{1,0:T(8,128)(2,1)} %collective-permute-done.1), channel_id=1, source_target_pairs={{0,4},{4,8},{8,12},{12,0},{1,5},{5,9},{9,13},{13,1},{2,6},{6,10},{... | collective-permute-start | bytes 6291464 | tf_op jit(solution)/shard_map/ppermute | solution.py:14
  313.4 46.9 %copy-start.2 = (bf16[512,2048]{1,0:T(8,128)(2,1)S(1)}, bf16[512,2048]{1,0:T(8,128)(2,1)}, u32[]{:S(2)}) copy-start(bf16[512,2048]{1,0:T(8,128)(2,1)} %copy-done.1) | copy-start | bytes 6291460
  363.4 9.5 %copy-start.3 = (bf16[256,2048]{1,0:T(8,128)(2,1)S(1)}, bf16[256,2048]{1,0:T(8,128)(2,1)}, u32[]{:S(2)}) copy-start(bf16[256,2048]{1,0:T(8,128)(2,1)} %all-gather.10.cloned.1.call-done) | copy-start | bytes 3145732
  373.0 41.3 %copy-start.4 = (bf16[256,512]{1,0:T(8,128)(2,1)S(1)}, bf16[256,512]{1,0:T(8,128)(2,1)}, u32[]{:S(2)}) copy-start(bf16[256,512]{1,0:T(8,128)(2,1)} %fusion.14) | copy-start | bytes 786436
Sparse Core Ops, SparseCore 0:
  8.9 19.4 all-gather.5
  29.9 45.6 all-gather.7
  79.1 15.4 all-gather.9
  96.0 216.7 all-gather.11
  384.9 29.3 reduce-scatter.1
